TPU v7x, 512 devices: a whole 4x4x16 slice. The times are simulated.
512 devices in a mesh: sp: 64 (over z, y), tp: 8 (over x, core).
Axes of the slice: x: 4, y: 4, z: 16, core: 2. Of those that a mesh axis runs over, the one named last changes fastest.
Arguments:
- target: bfloat16 [8192, 2048], P('sp'), may hold values from -0.375 to 0.375
- source: bfloat16 [16384, 2048], P(('sp', 'tp')), may hold values from -0.375 to 0.375
- target_gain: float32 [2048], replicated, may hold values from 0.3 to 12
- source_gain: float32 [2048], replicated, may hold values from 0.3 to 12
- w_query: bfloat16 [2048, 1024], P(None, 'tp'), may hold values from -0.125 to 0.125
- w_key: bfloat16 [2048, 256], replicated, may hold values from -0.125 to 0.125
- w_value: bfloat16 [2048, 256], replicated, may hold values from -0.125 to 0.125
- attended: bfloat16 [8192, 1024], P('sp', 'tp'), may hold values from -6 to 6
- d_attended: bfloat16 [8192, 1024], P('sp', 'tp'), may hold values from -24 to 24
Outputs:
- d_target: bfloat16 [8192, 2048], P('sp')
- d_source: float32 [16384, 2048], P(('sp', 'tp'))
- d_w_query: float32 [2048, 1024], P('sp', 'tp')
All inputs are finite; a program needn't handle non-finite values.
Results may differ from a plain program's by a relative error of at most 0.02.
The roundings to bfloat16 on the way count: a program that leaves them out, or rounds other values in their place, can miss the bound.
Values may be sent and summed in bfloat16 or wider, within the bound.
A program may use at most 64 MiB of HBM per device.

v0:
```python
import jax
import jax.numpy as jnp
from jax import lax
from jax.sharding import Mesh
from jax.sharding import PartitionSpec as P

KVH = 2
HD = 128
SP = ("sp_0", "sp_1")
SP_TP = ("sp_0", "sp_1", "tp")
EPS = 1e-06


def sent_together(arrays, axis, dim, along):
    widths = [a.shape[along] for a in arrays]
    both = jnp.concatenate(arrays, axis=along)
    result = lax.all_gather(both, axis, axis=dim, tiled=True)
    return tuple(jnp.split(result, [sum(widths[:k]) for k in range(1, len(widths))], axis=along))


def joined_all(shard, axes, combine):
    for axis in axes:
        pieces = jax.tree.map(lambda part: lax.all_gather(part, axis), shard)
        shard = jax.tree.map(lambda part: part[0], pieces)
        for k in range(1, lax.axis_size(axis)):
            shard = combine(shard, jax.tree.map(lambda part: part[k], pieces))
    return shard


def in_blocks(shard, dim, peers):
    shape = shard.shape
    pieces = shard.reshape(*shape[:dim], peers, shape[dim] // peers, *shape[dim + 1 :])
    return jnp.moveaxis(pieces, dim, 0)


def sent_and_summed(shard, axis, dim):
    pieces = in_blocks(shard, dim, lax.axis_size(axis))
    arrived = lax.all_to_all(pieces, axis, split_axis=0, concat_axis=0, tiled=True)
    return arrived.sum(axis=0)


def summed_on_arrival(shard, axis, dim):
    peers = lax.axis_size(axis)
    pieces = lax.all_to_all(in_blocks(shard, dim, peers), axis, 0, 0, tiled=True)
    return jnp.sum(pieces.astype(jnp.float32), axis=0)


def joined_along(pieces, dim):
    pieces = jnp.moveaxis(pieces, 0, dim)
    shape = pieces.shape
    return pieces.reshape(*shape[:dim], shape[dim] * shape[dim + 1], *shape[dim + 2 :])


def copy_for_each(shard, axis):
    peers = lax.axis_size(axis)
    return lax.all_to_all(
        jnp.broadcast_to(shard[None], (peers, *shard.shape)), axis, 0, 0, tiled=True
    )


def gathered_copies(shard, axis, dim):
    return joined_along(copy_for_each(shard, axis), dim)


def norm_rows(matrix, gain_vector):
    widened = matrix.astype(jnp.float32)
    inverse = lax.rsqrt(jnp.mean(widened * widened, axis=-1, keepdims=True) + EPS)
    return widened * inverse * gain_vector


def norm_back(matrix, gain_vector, cotangent):
    _, pullback = jax.vjp(lambda values: norm_rows(values, gain_vector), matrix.astype(jnp.float32))
    return pullback(cotangent)[0]


def block_count(row_count, most_rows):
    number = 1
    while row_count % (number * 2) == 0 and row_count // number > most_rows:
        number = number * 2
    return number


def merge_totals(earlier, latter):
    maxima = jnp.maximum(earlier[0], latter[0])
    totals = earlier[1] * jnp.exp(earlier[0] - maxima) + latter[1] * jnp.exp(latter[0] - maxima)
    return (maxima, totals)


def block_totals(queries, key_head, scaling):
    row_count = queries.shape[0]
    per_head = queries.reshape(row_count, -1, key_head.shape[1])
    scores = (
        jnp.einsum("rhd,sd->rhs", per_head, key_head, preferred_element_type=jnp.float32) * scaling
    )
    maxima = jnp.max(scores, axis=-1)
    totals = jnp.sum(jnp.exp(scores - maxima[..., None]), axis=-1)
    return (maxima, totals)


def score_grads(query_heads, grad_heads, delta_rows, log_total, key_head, value_head, scaling):
    scores = (
        jnp.einsum("rhd,sd->rhs", query_heads, key_head, preferred_element_type=jnp.float32)
        * scaling
    )
    weights = jnp.exp(scores - log_total[..., None])
    d_weights = jnp.einsum(
        "rhd,sd->rhs", grad_heads, value_head, preferred_element_type=jnp.float32
    )
    d_scores = (weights * (d_weights - delta_rows.astype(jnp.float32)[..., None])).astype(
        jnp.bfloat16
    )
    return (weights, d_scores)


def gradient_block(carried, blocks, key_head, value_head, scaling):
    key_acc, value_acc = carried
    queries, cotangent, delta_rows, log_total = blocks
    row_count = queries.shape[0]
    head_dim = key_head.shape[1]
    query_heads = queries.reshape(row_count, -1, head_dim)
    grad_heads = cotangent.reshape(row_count, -1, head_dim)
    weights, d_scores = score_grads(
        query_heads, grad_heads, delta_rows, log_total, key_head, value_head, scaling
    )
    key_acc = (
        key_acc
        + jnp.einsum("rhs,rhd->sd", d_scores, query_heads, preferred_element_type=jnp.float32)
        * scaling
    )
    value_acc = value_acc + jnp.einsum(
        "rhs,rhd->sd", weights.astype(jnp.bfloat16), grad_heads, preferred_element_type=jnp.float32
    )
    return ((key_acc, value_acc), None)


def local(target, source, target_gain, source_gain, w_query, w_key, w_value, attended, d_attended):
    tp_size = lax.axis_size("tp")
    local_rows = target.shape[0]
    source_rows = source.shape[0]
    query_width = w_query.shape[1]
    scaling = HD ** (-0.5)
    normed_target = norm_rows(target, target_gain).astype(jnp.bfloat16)
    normed_source = norm_rows(source, source_gain).astype(jnp.bfloat16)
    query = jnp.dot(normed_target, w_query, preferred_element_type=jnp.float32).astype(jnp.bfloat16)
    key_own = jnp.dot(normed_source, w_key, preferred_element_type=jnp.float32).astype(jnp.bfloat16)
    value_own = jnp.dot(normed_source, w_value, preferred_element_type=jnp.float32).astype(
        jnp.bfloat16
    )
    key_block, value_block = sent_together((key_own, value_own), "tp", 0, 1)
    group_size = tp_size // KVH
    kv_index = lax.axis_index("tp") // group_size
    key_head = lax.dynamic_slice_in_dim(key_block, kv_index * HD, HD, 1)
    value_head = lax.dynamic_slice_in_dim(value_block, kv_index * HD, HD, 1)
    delta = jnp.einsum(
        "rhd,rhd->rh",
        d_attended.reshape(local_rows, -1, HD),
        attended.reshape(local_rows, -1, HD),
        preferred_element_type=jnp.float32,
    ).astype(jnp.bfloat16)
    all_queries = lax.all_gather(query, SP, axis=0, tiled=True)
    target_total = all_queries.shape[0]
    number = block_count(target_total, 512)
    maxima, totals = lax.map(
        lambda blocked: block_totals(blocked, key_head, scaling),
        all_queries.reshape(number, target_total // number, query_width),
    )
    maxima = maxima.reshape(target_total, -1)
    totals = totals.reshape(target_total, -1)
    maxima, totals = joined_all((maxima, totals), SP, merge_totals)
    log_total = maxima + jnp.log(totals)
    block_rows = key_head.shape[0]
    start_state = (
        jnp.zeros((block_rows, HD), jnp.float32),
        jnp.zeros((block_rows, HD), jnp.float32),
    )
    key_acc = start_state[0]
    value_acc = start_state[1]
    cotangent, delta_piece = sent_together((d_attended, delta), SP, 0, 1)
    row_count = cotangent.shape[0]
    pieces_count = block_count(row_count, 512)
    blocked = tuple(
        (
            member.reshape((pieces_count, row_count // pieces_count) + member.shape[1:])
            for member in (all_queries, cotangent, delta_piece, log_total)
        )
    )

    def fold_inner_step(state, blocks):
        return gradient_block(state, blocks, key_head, value_head, scaling)

    (key_acc, value_acc), grad_rows = lax.scan(fold_inner_step, (key_acc, value_acc), blocked)
    folded = (key_acc, value_acc)
    key_acc = folded[0]
    value_acc = folded[1]
    own_totals = lax.dynamic_slice_in_dim(log_total, lax.axis_index(SP) * local_rows, local_rows, 0)
    own_queries = query.reshape(local_rows, -1, HD)
    own_grads = d_attended.reshape(local_rows, -1, HD)
    query_start = jnp.zeros((local_rows, query_width // HD, HD), jnp.float32)
    keys_piece, values_piece = sent_together((key_head, value_head), SP, 0, 1)
    row_count = keys_piece.shape[0]
    pieces_count = block_count(row_count, 512)
    key_blocks = keys_piece.reshape(pieces_count, row_count // pieces_count, HD)
    value_blocks = values_piece.reshape(pieces_count, row_count // pieces_count, HD)

    def key_inner_step(state, blocks):
        keys_now, values_now = blocks
        _, d_scores = score_grads(
            own_queries, own_grads, delta, own_totals, keys_now, values_now, scaling
        )
        return (
            state
            + jnp.einsum("rhs,sd->rhd", d_scores, keys_now, preferred_element_type=jnp.float32)
            * scaling,
            None,
        )

    result, _ = lax.scan(key_inner_step, query_start, (key_blocks, value_blocks))
    d_query = result.reshape(local_rows, query_width).astype(jnp.bfloat16)
    d_w_query = sent_and_summed(
        jnp.einsum("rd,rc->dc", normed_target, d_query, preferred_element_type=jnp.float32), SP, 0
    )
    share_rows = local_rows // tp_size
    grad_rows = d_query
    d_normed = summed_on_arrival(
        jnp.einsum("rc,dc->rd", grad_rows, w_query, preferred_element_type=jnp.float32).astype(
            jnp.bfloat16
        ),
        "tp",
        0,
    )
    own_rows = lax.dynamic_slice_in_dim(target, lax.axis_index("tp") * share_rows, share_rows, 0)
    own_grad = norm_back(own_rows, target_gain, d_normed).astype(jnp.bfloat16)
    d_target = gathered_copies(own_grad, "tp", 0)
    stacked = jnp.stack([key_acc, value_acc], axis=1).reshape(tp_size, source_rows, 2 * HD)
    returned = lax.all_to_all(
        stacked.astype(jnp.bfloat16), "tp", split_axis=0, concat_axis=0, tiled=True
    ).astype(stacked.dtype)
    grouped = returned.reshape(KVH, group_size, source_rows, 2, HD).sum(axis=1)
    d_key = (
        grouped[:, :, 0, :].transpose(1, 0, 2).reshape(source_rows, KVH * HD).astype(jnp.bfloat16)
    )
    d_value = (
        grouped[:, :, 1, :].transpose(1, 0, 2).reshape(source_rows, KVH * HD).astype(jnp.bfloat16)
    )
    d_normed_source = jnp.einsum(
        "rc,dc->rd", d_key, w_key, preferred_element_type=jnp.float32
    ) + jnp.einsum("rc,dc->rd", d_value, w_value, preferred_element_type=jnp.float32)
    d_source = norm_back(source, source_gain, d_normed_source)
    return (d_target, d_source, d_w_query)


def solution(mesh):
    finer = Mesh(mesh.devices.reshape(16, 4, mesh.shape["tp"]), ("sp_0", "sp_1", "tp"))
    placed = (
        P(SP, None),
        P(SP_TP, None),
        P(),
        P(),
        P(None, "tp"),
        P(),
        P(),
        P(SP, "tp"),
        P(SP, "tp"),
    )
    return jax.shard_map(
        local,
        mesh=finer,
        in_specs=placed,
        out_specs=(P(SP, None), P(SP_TP, None), P(SP, "tp")),
        check_vma=False,
    )
```

profile of v0, /device:TPU:8, one launch (start us, length us, event | category | flops | bytes accessed | tf_op | source)
XLA Modules:
  0.0 659.4 jit_solution(8378921525425368850)
XLA Ops:
  10.1 2.0 convolution_convert_fusion.1
  17.0 13.2 %all_gather.26 = bf16[256,512]{1,0:T(8,128)(2,1)S(1)} all-gather(bf16[32,512]{1,0:T(8,128)(2,1)S(1)} %pad_maximum_fusion.3), channel_id=1, replica_groups=mesh['sp_0'=16,'sp_1'=4,'tp'=8] {'tp'}, dimensions={0}, use_global_device_ids=true | all-gather | bytes 294912 | tf_op jit(solution)/shard_map/all_gather | solution.py:17
  31.0 125.5 %all-gather.6.cloned.1.call-done = bf16[8192,128]{1,0:T(8,128)(2,1)} async-done(((bf16[128,128]{1,0:T(8,128)(2,1)}), bf16[8192,128]{1,0:T(8,128)(2,1)}) %all-gather.6.cloned.1.call-update) | async-done | bytes 2097168 | tf_op jit(solution)/shard_map/all_gather | solution.py:160
  156.5 20.6 %while.36 = (s32[]{:T(128)}, f32[16,512,1]{1,2,0:T(1,128)S(1)}, f32[16,512,1]{1,2,0:T(1,128)S(1)}, bf16[16,512,128]{2,1,0:T(8,128)(2,1)}, bf16[256,128]{1,0:T(8,128)(2,1)S(1)}, /*index=5*/s32[]{:T(128)}) while((s32[]{:T(128)}, f32[16,512,1]{1,2,0:T(1,128)S(1)}, f32[16,512,1]{1,2,0:T(1,128)S(1)}, bf16[16,512,128]{2,1,0:T(8,128)(2,1)}, ...), condition=%wide.region_5.6_spmd, body=%wide.region_2.5_spmd.sunk | while | flops 34077696 | bytes 1259605 | solution.py:163
  177.1 31.7 %all_gather.31 = f32[16,8192,1]{1,2,0:T(1,128)S(1)} all-gather(f32[1,8192,1]{1,2,0:T(1,128)S(1)} %bitcast.234), channel_id=1, replica_groups=mesh['sp_0'=16,'sp_1'=4,'tp'=8] {'sp_0'}, dimensions={0}, use_global_device_ids=true | all-gather | bytes 557056 | tf_op jit(solution)/shard_map/all_gather | solution.py:23
  208.8 29.3 %all_gather.29 = f32[16,8192,1]{1,2,0:T(1,128)S(1)} all-gather(f32[1,8192,1]{1,2,0:T(1,128)} %bitcast.233), channel_id=1, replica_groups=mesh['sp_0'=16,'sp_1'=4,'tp'=8] {'sp_0'}, dimensions={0}, use_global_device_ids=true | all-gather | bytes 557056 | tf_op jit(solution)/shard_map/all_gather | solution.py:23
  239.6 12.6 %all_gather.30 = f32[4,8192,1]{1,2,0:T(1,128)S(1)} all-gather(f32[1,8192,1]{1,2,0:T(1,128)S(1)} %get-tuple-element.240), channel_id=1, replica_groups=mesh['sp_0'=16,'sp_1'=4,'tp'=8] {'sp_1'}, dimensions={0}, use_global_device_ids=true | all-gather | bytes 163840 | tf_op jit(solution)/shard_map/all_gather | solution.py:23
  252.3 12.1 %all_gather.32 = f32[4,8192,1]{1,2,0:T(1,128)S(1)} all-gather(f32[1,8192,1]{1,2,0:T(1,128)S(1)} %get-tuple-element.239), channel_id=1, replica_groups=mesh['sp_0'=16,'sp_1'=4,'tp'=8] {'sp_1'}, dimensions={0}, use_global_device_ids=true | all-gather | bytes 163840 | tf_op jit(solution)/shard_map/all_gather | solution.py:23
  265.3 36.0 %all-gather.8.cloned.1.call-done = bf16[8192,129]{1,0:T(8,128)(2,1)} async-done(((bf16[128,129]{1,0:T(8,128)(2,1)}), bf16[8192,129]{1,0:T(8,128)(2,1)}) %all-gather.8.cloned.1.call-update) | async-done | bytes 2113552 | tf_op jit(solution)/shard_map/all_gather | solution.py:17
  301.3 2.2 slice_reduce_fusion
  304.1 3.0 split.28
  307.2 84.5 %while.38 = (s32[]{:T(128)}, f32[256,128]{1,0:T(8,128)S(1)}, f32[256,128]{1,0:T(8,128)S(1)}, bf16[16,512,128]{2,1,0:T(8,128)(2,1)}, bf16[256,128]{1,0:T(8,128)(2...) while((s32[]{:T(128)}, f32[256,128]{1,0:T(8,128)S(1)}, ...), condition=%wide.region_12.13_spmd.clone, body=%wide.region_11.12_spmd.clone.sunk | while | flops 135168512 | bytes 2765455 | solution.py:191
  391.7 64.3 %all-gather.4.cloned.1.call-done = bf16[16384,256]{1,0:T(8,128)(2,1)} async-done(((bf16[256,256]{1,0:T(8,128)(2,1)}), bf16[16384,256]{1,0:T(8,128)(2,1)}) %all-gather.4.cloned.1.call-update) | async-done | bytes 8388624 | tf_op jit(solution)/shard_map/all_gather | solution.py:17
  456.0 5.7 fusion.125
  461.8 81.4 %while.37 = (s32[]{:T(128)}, f32[128,1,128]{2,0,1:T(8,128)S(1)}, bf16[32,512,128]{2,1,0:T(8,128)(2,1)}, bf16[128,1,128]{2,0,1:T(8,128)(2,1)S(1)}, f32[128,1]{0,1...) while((s32[]{:T(128)}, f32[128,1,128]{2,0,1:T(8,128)S(1)}, ...), condition=%wide.region_7.8_spmd.clone, body=%wide.region_6.7_spmd.clone.sunk | while | flops 50708608 | bytes 1117562 | solution.py:217
  543.2 2.1 convolution_convert_fusion
  545.3 4.3 all-to-all-start
  550.5 9.5 %all-to-all-done = bf16[8,16,2048]{2,1,0:T(8,128)(2,1)} async-done(((bf16[8,16,2048]{2,1,0:T(8,128)(2,1)}), bf16[8,16,2048]{2,1,0:T(8,128)(2,1)}, u32[]{:S(2)}, u32[]{:S(2)}) %all-to-all-start) | async-done | bytes 524320 | tf_op jit(solution)/shard_map/all_to_all | solution.py:44
  560.0 3.4 all-to-all-start.2
  566.5 2.9 all-to-all-done.2
  570.2 4.3 all-to-all-start.1
  575.8 9.1 %all-to-all-done.1 = bf16[8,16,2048]{2,1,0:T(8,128)(2,1)} async-done(((bf16[8,16,2048]{2,1,0:T(8,128)(2,1)}), bf16[8,16,2048]{2,1,0:T(8,128)(2,1)}, u32[]{:S(2)}, u32[]{:S(2)}) %all-to-all-start.1) | async-done | bytes 524320 | tf_op jit(solution)/shard_map/all_to_all | solution.py:56
  584.9 10.6 %all-to-all-start.3 = ((f32[64,32,128]{2,1,0:T(8,128)}), f32[64,32,128]{2,1,0:T(8,128)S(1)}, u32[]{:S(2)}, u32[]{:S(2)}) async-start(f32[64,32,128]{2,1,0:T(8,128)} %fusion.92), calls=%async_computation.3 | async-start | bytes 2097152 | tf_op jit(solution)/shard_map/all_to_all | solution.py:38
  598.4 51.9 %all-to-all-done.3 = f32[64,32,128]{2,1,0:T(8,128)S(1)} async-done(((f32[64,32,128]{2,1,0:T(8,128)}), f32[64,32,128]{2,1,0:T(8,128)S(1)}, u32[]{:S(2)}, u32[]{:S(2)}) %all-to-all-start.3) | async-done | bytes 1048608 | tf_op jit(solution)/shard_map/all_to_all | solution.py:38
  (313 shorter events, 207.4 us)
Async XLA Ops:
  7.2 9.1 %copy-start = (bf16[2048,256]{1,0:T(8,128)(2,1)S(1)}, bf16[2048,256]{1,0:T(8,128)(2,1)}, u32[]{:S(2)}) copy-start(bf16[2048,256]{1,0:T(8,128)(2,1)} %param.21) | copy-start | bytes 3145732
  7.2 9.1 %copy-start.2 = (bf16[32,2048]{1,0:T(8,128)(2,1)S(1)}, bf16[32,2048]{1,0:T(8,128)(2,1)}, u32[]{:S(2)}) copy-start(bf16[32,2048]{1,0:T(8,128)(2,1)} %param.16) | copy-start | bytes 393220
  7.2 9.1 %copy-start.8 = (f32[2048]{0:T(1024)S(1)}, f32[2048]{0:T(1024)}, u32[]{:S(2)}) copy-start(f32[2048]{0:T(1024)} %param.18) | copy-start | bytes 24580
  7.2 9.4 %copy-start.1 = (bf16[2048,256]{1,0:T(8,128)(2,1)S(1)}, bf16[2048,256]{1,0:T(8,128)(2,1)}, u32[]{:S(2)}) copy-start(bf16[2048,256]{1,0:T(8,128)(2,1)} %param.20) | copy-start | bytes 3145732
  7.2 149.3 %all-gather.6.cloned.1.call-start = ((), (), s32[]{:S(2)}) async-start(), calls=%async_computation.5 | async-start | bytes 2129920 | tf_op jit(solution)/shard_map/all_gather | solution.py:160
  12.1 289.2 %all-gather.8.cloned.1.call-start = ((), (), s32[]{:S(2)}) async-start(), calls=%async_computation.6 | async-start | bytes 4259840 | tf_op jit(solution)/shard_map/all_gather | solution.py:17
  13.0 2.7 copy-start.13
  14.6 441.5 %all-gather.4.cloned.1.call-start = ((), (), s32[]{:S(2)}) async-start(), calls=%async_computation.4 | async-start | bytes 8519680 | tf_op jit(solution)/shard_map/all_gather | solution.py:17
  15.7 0.6 copy-start.15
  16.3 13.9 %copy-start.11 = (f32[32]{0:T(128)}, f32[32]{0:T(128)S(1)}, u32[]{:S(2)}) copy-start(f32[32]{0:T(128)S(1)} %fusion.122) | copy-start | bytes 388
  177.1 31.8 %copy-start.10 = (f32[16,512,1]{1,2,0:T(1,128)}, f32[16,512,1]{1,2,0:T(1,128)S(1)}, u32[]{:S(2)}) copy-start(f32[16,512,1]{1,2,0:T(1,128)S(1)} %get-tuple-element.121) | copy-start | bytes 98308
  391.7 70.1 %copy-start.4 = (f32[128,1,128]{2,0,1:T(8,128)S(1)}, f32[128,1,128]{2,0,1:T(8,128)}, u32[]{:S(2)}) copy-start(f32[128,1,128]{2,0,1:T(8,128)} %custom-call) | copy-start | bytes 196612
  391.7 70.0 %copy-start.5 = (bf16[128,128]{1,0:T(8,128)(2,1)S(1)}, bf16[128,128]{1,0:T(8,128)(2,1)}, u32[]{:S(2)}) copy-start(bf16[128,128]{1,0:T(8,128)(2,1)} %convolution_convert_fusion.1) | copy-start | bytes 98308
  391.7 70.0 %copy-start.6 = (bf16[128,128]{1,0:T(8,128)(2,1)S(1)}, bf16[128,128]{1,0:T(8,128)(2,1)}, u32[]{:S(2)}) copy-start(bf16[128,128]{1,0:T(8,128)(2,1)} %param.23) | copy-start | bytes 98308
  391.7 70.0 %copy-start.14 = (bf16[128]{0:T(256)(128)(2,1)S(1)}, bf16[128]{0:T(256)(128)(2,1)}, u32[]{:S(2)}) copy-start(bf16[128]{0:T(256)(128)(2,1)} %copy-done.13) | copy-start | bytes 772
  461.8 102.8 %copy-start.9 = (f32[2048]{0:T(1024)S(1)}, f32[2048]{0:T(1024)}, u32[]{:S(2)}) copy-start(f32[2048]{0:T(1024)} %param.17) | copy-start | bytes 24580
  545.3 14.7 %all-to-all-start = ((bf16[8,16,2048]{2,1,0:T(8,128)(2,1)}), bf16[8,16,2048]{2,1,0:T(8,128)(2,1)}, u32[]{:S(2)}, u32[]{:S(2)}) async-start(bf16[8,16,2048]{2,1,0:T(8,128)(2,1)} %bitcast.217), calls=%async_computation | async-start | bytes 1048576 | tf_op jit(solution)/shard_map/all_to_all | solution.py:44
  560.0 9.4 %all-to-all-start.2 = ((bf16[8,32,256]{2,1,0:T(8,128)(2,1)}), bf16[8,32,256]{2,1,0:T(8,128)(2,1)S(1)}, u32[]{:S(2)}, u32[]{:S(2)}) async-start(bf16[8,32,256]{2,1,0:T(8,128)(2,1)} %convert_element_type.121), calls=%async_computation.2 | async-start | bytes 262144 | tf_op jit(solution)/shard_map/all_to_all | solution.py:235
  563.4 33.6 %copy-start.3 = (bf16[32,2048]{1,0:T(8,128)(2,1)S(1)}, bf16[32,2048]{1,0:T(8,128)(2,1)}, u32[]{:S(2)}) copy-start(bf16[32,2048]{1,0:T(8,128)(2,1)} %param.16) | copy-start | bytes 393220
  569.4 15.5 %copy-start.7 = (bf16[8,32,256]{2,1,0:T(8,128)(2,1)}, bf16[8,32,256]{2,1,0:T(8,128)(2,1)S(1)}, u32[]{:S(2)}) copy-start(bf16[8,32,256]{2,1,0:T(8,128)(2,1)S(1)} %all-to-all-done.2) | copy-start | bytes 393220
  570.2 27.3 %copy-start.16 = (f32[32]{0:T(128)S(1)}, f32[32]{0:T(128)}, u32[]{:S(2)}) copy-start(f32[32]{0:T(128)} %copy-done.15) | copy-start | bytes 388
  570.2 27.3 %copy-start.12 = (f32[32]{0:T(128)S(1)}, f32[32]{0:T(128)}, u32[]{:S(2)}) copy-start(f32[32]{0:T(128)} %copy-done.11) | copy-start | bytes 388
  570.2 14.6 %all-to-all-start.1 = ((bf16[8,16,2048]{2,1,0:T(8,128)(2,1)}), bf16[8,16,2048]{2,1,0:T(8,128)(2,1)}, u32[]{:S(2)}, u32[]{:S(2)}) async-start(bf16[8,16,2048]{2,1,0:T(8,128)(2,1)} %broadcast_in_dim.22), calls=%async_computation.1 | async-start | bytes 1048576 | tf_op jit(solution)/shard_map/all_to_all | solution.py:56
  584.9 65.5 %all-to-all-start.3 = ((f32[64,32,128]{2,1,0:T(8,128)}), f32[64,32,128]{2,1,0:T(8,128)S(1)}, u32[]{:S(2)}, u32[]{:S(2)}) async-start(f32[64,32,128]{2,1,0:T(8,128)} %fusion.92), calls=%async_computation.3 | async-start | bytes 2097152 | tf_op jit(solution)/shard_map/all_to_all | solution.py:38
Sparse Core Ops, SparseCore 0:
  12.2 144.2 all-gather.5
  159.4 141.8 all-gather.7
  304.8 151.1 all-gather.3
where the time goes:
time: 664 us; the launch traced here: 659 us
  waiting for transfers between devices  299 us (45%)
  matrix products  167 us (25%)
  blocking collectives  98.9 us (15%)
  local copies, waits for them, and re-layouts  29.6 us (4%)
  other arithmetic  25.7 us (4%)
  starting transfers between devices  22.6 us (3%)
  between operations  14.2 us (2%)
    all_gather x1, waiting for transfers between devices, local(): all_queries = lax.all_gather(query, SP, axis=0, tiled=True)  125 us
    all_gather x2, waiting for transfers between devices, sent_together(): result = lax.all_gather(both, axis, axis=dim, tiled=True)  100 us
    all_gather x4, blocking collectives, joined_all(): pieces = jax.tree.map(lambda part: lax.all_gather(part, axis), shard)  85.7 us
    dot_general x48, matrix products, score_grads(): jnp.einsum('rhd,sd->rhs', query_heads, key_head, preferred_element_type=j...  53.8 us
    all_to_all x1, waiting for transfers between devices, sent_and_summed(): lax.all_to_all(pieces, axis, split_axis=0, concat_axis=0, tiled=True)  51.9 us
    dot_general x32, matrix products, key_inner_step(): jnp.einsum('rhs,sd->rhd', d_scores, keys_now, preferred_element_type=jnp....  44.5 us
    dot_general x16, matrix products, gradient_block(): jnp.einsum('rhs,rhd->sd', d_scores, query_heads, preferred_element_type=j...  24.1 us
    dot_general x16, matrix products, gradient_block(): jnp.einsum('rhs,rhd->sd', weights.astype(jnp.bfloat16), grad_heads, prefe...  19.2 us
  transfers between devices with their start and end apart: 7, of which 7 were waited for; matrix products, arithmetic and copies ran while one was open for 19% of the time, Pallas kernels for 0%

commit v1 on v0

--- a/solution.py
+++ b/solution.py
@@ -157,7 +157,10 @@
         attended.reshape(local_rows, -1, HD),
         preferred_element_type=jnp.float32,
     ).astype(jnp.bfloat16)
-    all_queries = lax.all_gather(query, SP, axis=0, tiled=True)
+    upper = jax.lax.axis_size(SP)
+    after = jnp.stack([query] * upper, 0)
+    block_next = jax.lax.all_to_all(after, SP, split_axis=0, concat_axis=0)
+    all_queries = jnp.concatenate(block_next, 0)
     target_total = all_queries.shape[0]
     number = block_count(target_total, 512)
     maxima, totals = lax.map(

time: 664 us -> 608 us (0.916)
  waiting for transfers between devices: 299 us -> 222 us
  starting transfers between devices: 22.6 us -> 41.8 us
    all_gather x1 -> x0, waiting for transfers between devices: 125 us -> none  [local(): all_queries = lax.all_gather(query, SP, axis=0, tiled=True)]
    all_gather x2, waiting for transfers between devices: 100 us -> 149 us  [sent_together(): result = lax.all_gather(both, axis, axis=dim, tiled=True)]
    all_to_all x0 -> x1, starting transfers between devices: none -> 18.9 us  [local(): block_next = jax.lax.all_to_all(after, SP, split_axis=0, concat_axis=0)]
  transfers between devices with their start and end apart: 7 -> 7, of which waited for: 7 -> 5; matrix products, arithmetic and copies ran while one was open for 19% -> 20% of each run, Pallas kernels for 0% -> 0%
where the time goes in v1:
time: 608 us; the launch traced here: 604 us
  waiting for transfers between devices  222 us (37%)
  matrix products  166 us (27%)
  blocking collectives  101 us (17%)
  starting transfers between devices  41.8 us (7%)
  local copies, waits for them, and re-layouts  32 us (5%)
  other arithmetic  23.3 us (4%)
  between operations  14.5 us (2%)
    all_gather x2, waiting for transfers between devices, sent_together(): result = lax.all_gather(both, axis, axis=dim, tiled=True)  149 us
    all_gather x4, blocking collectives, joined_all(): pieces = jax.tree.map(lambda part: lax.all_gather(part, axis), shard)  87.6 us
    dot_general x48, matrix products, score_grads(): jnp.einsum('rhd,sd->rhs', query_heads, key_head, preferred_element_type=j...  53.7 us
    all_to_all x1, waiting for transfers between devices, sent_and_summed(): lax.all_to_all(pieces, axis, split_axis=0, concat_axis=0, tiled=True)  51.9 us
    dot_general x32, matrix products, key_inner_step(): jnp.einsum('rhs,sd->rhd', d_scores, keys_now, preferred_element_type=jnp....  44.5 us
    dot_general x16, matrix products, gradient_block(): jnp.einsum('rhs,rhd->sd', d_scores, query_heads, preferred_element_type=j...  24.1 us
    dot_general x16, matrix products, gradient_block(): jnp.einsum('rhs,rhd->sd', weights.astype(jnp.bfloat16), grad_heads, prefe...  19.2 us
    all_to_all x1, starting transfers between devices, local(): block_next = jax.lax.all_to_all(after, SP, split_axis=0, concat_axis=0)  18.9 us
  transfers between devices with their start and end apart: 7, of which 5 were waited for; matrix products, arithmetic and copies ran while one was open for 20% of the time, Pallas kernels for 0%

profile of v1, /device:TPU:8, one launch (start us, length us, event | category | flops | bytes accessed | tf_op | source)
XLA Modules:
  0.0 603.5 jit_solution(10714220270812947956)
XLA Ops:
  12.0 1.8 stack.11
  13.8 18.9 %all-to-all-start = ((bf16[64,128,128]{2,1,0:T(8,128)(2,1)}), bf16[64,128,128]{2,1,0:T(8,128)(2,1)}, u32[]{:S(2)}, u32[]{:S(2)}) async-start(bf16[64,128,128]{2,1,0:T(8,128)(2,1)} %stack.11), calls=%async_computation | async-start | bytes 4194304 | tf_op jit(solution)/shard_map/all_to_all | solution.py:162
  35.3 13.2 %all_gather.23 = bf16[256,512]{1,0:T(8,128)(2,1)S(1)} all-gather(bf16[32,512]{1,0:T(8,128)(2,1)S(1)} %pad_maximum_fusion.3), channel_id=1, replica_groups=mesh['sp_0'=16,'sp_1'=4,'tp'=8] {'tp'}, dimensions={0}, use_global_device_ids=true | all-gather | bytes 294912 | tf_op jit(solution)/shard_map/all_gather | solution.py:17
  49.3 149.0 %all-gather.5.cloned.1.call-done = bf16[8192,129]{1,0:T(8,128)(2,1)} async-done(((bf16[128,129]{1,0:T(8,128)(2,1)}), bf16[8192,129]{1,0:T(8,128)(2,1)}) %all-gather.5.cloned.1.call-update) | async-done | bytes 2113552 | tf_op jit(solution)/shard_map/all_gather | solution.py:17
  198.3 2.2 slice_reduce_fusion
  201.2 3.0 split.28
  204.2 20.6 %while.36 = (s32[]{:T(128)}, f32[16,512,1]{1,2,0:T(1,128)S(1)}, f32[16,512,1]{1,2,0:T(1,128)S(1)}, bf16[16,512,128]{2,1,0:T(8,128)(2,1)}, bf16[256,128]{1,0:T(8,128)(2,1)S(1)}, /*index=5*/s32[]{:T(128)}) while((s32[]{:T(128)}, f32[16,512,1]{1,2,0:T(1,128)S(1)}, f32[16,512,1]{1,2,0:T(1,128)S(1)}, bf16[16,512,128]{2,1,0:T(8,128)(2,1)}, ...), condition=%wide.region_5.6_spmd, body=%wide.region_2.5_spmd.sunk | while | flops 34077696 | bytes 1259605 | solution.py:166
  224.8 32.4 %all_gather.27 = f32[16,8192,1]{1,2,0:T(1,128)S(1)} all-gather(f32[1,8192,1]{1,2,0:T(1,128)S(1)} %bitcast.233), channel_id=1, replica_groups=mesh['sp_0'=16,'sp_1'=4,'tp'=8] {'sp_0'}, dimensions={0}, use_global_device_ids=true | all-gather | bytes 557056 | tf_op jit(solution)/shard_map/all_gather | solution.py:23
  257.2 30.1 %all_gather.25 = f32[16,8192,1]{1,2,0:T(1,128)S(1)} all-gather(f32[1,8192,1]{1,2,0:T(1,128)} %bitcast.232), channel_id=1, replica_groups=mesh['sp_0'=16,'sp_1'=4,'tp'=8] {'sp_0'}, dimensions={0}, use_global_device_ids=true | all-gather | bytes 557056 | tf_op jit(solution)/shard_map/all_gather | solution.py:23
  288.8 12.6 %all_gather.26 = f32[4,8192,1]{1,2,0:T(1,128)S(1)} all-gather(f32[1,8192,1]{1,2,0:T(1,128)S(1)} %get-tuple-element.240), channel_id=1, replica_groups=mesh['sp_0'=16,'sp_1'=4,'tp'=8] {'sp_1'}, dimensions={0}, use_global_device_ids=true | all-gather | bytes 163840 | tf_op jit(solution)/shard_map/all_gather | solution.py:23
  301.5 12.5 %all_gather.28 = f32[4,8192,1]{1,2,0:T(1,128)S(1)} all-gather(f32[1,8192,1]{1,2,0:T(1,128)S(1)} %get-tuple-element.239), channel_id=1, replica_groups=mesh['sp_0'=16,'sp_1'=4,'tp'=8] {'sp_1'}, dimensions={0}, use_global_device_ids=true | all-gather | bytes 163840 | tf_op jit(solution)/shard_map/all_gather | solution.py:23
  314.9 84.5 %while.38 = (s32[]{:T(128)}, f32[256,128]{1,0:T(8,128)S(1)}, f32[256,128]{1,0:T(8,128)S(1)}, bf16[16,512,128]{2,1,0:T(8,128)(2,1)}, bf16[256,128]{1,0:T(8,128)(2...) while((s32[]{:T(128)}, f32[256,128]{1,0:T(8,128)S(1)}, ...), condition=%wide.region_12.13_spmd.clone, body=%wide.region_11.12_spmd.clone.sunk | while | flops 135168512 | bytes 2765455 | solution.py:194
  399.5 5.7 fusion.125
  405.3 81.4 %while.37 = (s32[]{:T(128)}, f32[128,1,128]{2,0,1:T(8,128)S(1)}, bf16[32,512,128]{2,1,0:T(8,128)(2,1)}, bf16[128,1,128]{2,0,1:T(8,128)(2,1)S(1)}, f32[128,1]{0,1...) while((s32[]{:T(128)}, f32[128,1,128]{2,0,1:T(8,128)S(1)}, ...), condition=%wide.region_7.8_spmd.clone, body=%wide.region_6.7_spmd.clone.sunk | while | flops 50708608 | bytes 1117562 | solution.py:220
  486.6 2.1 convolution_convert_fusion
  488.8 4.2 all-to-all-start.1
  493.9 9.5 %all-to-all-done.1 = bf16[8,16,2048]{2,1,0:T(8,128)(2,1)} async-done(((bf16[8,16,2048]{2,1,0:T(8,128)(2,1)}), bf16[8,16,2048]{2,1,0:T(8,128)(2,1)}, u32[]{:S(2)}, u32[]{:S(2)}) %all-to-all-start.1) | async-done | bytes 524320 | tf_op jit(solution)/shard_map/all_to_all | solution.py:44
  503.4 3.4 all-to-all-start.3
  509.9 2.9 all-to-all-done.3
  513.6 4.3 all-to-all-start.2
  519.2 9.1 %all-to-all-done.2 = bf16[8,16,2048]{2,1,0:T(8,128)(2,1)} async-done(((bf16[8,16,2048]{2,1,0:T(8,128)(2,1)}), bf16[8,16,2048]{2,1,0:T(8,128)(2,1)}, u32[]{:S(2)}, u32[]{:S(2)}) %all-to-all-start.2) | async-done | bytes 524320 | tf_op jit(solution)/shard_map/all_to_all | solution.py:56
  528.3 11.0 %all-to-all-start.4 = ((f32[64,32,128]{2,1,0:T(8,128)}), f32[64,32,128]{2,1,0:T(8,128)S(1)}, u32[]{:S(2)}, u32[]{:S(2)}) async-start(f32[64,32,128]{2,1,0:T(8,128)} %fusion.92), calls=%async_computation.4 | async-start | bytes 2097152 | tf_op jit(solution)/shard_map/all_to_all | solution.py:38
  542.2 51.9 %all-to-all-done.4 = f32[64,32,128]{2,1,0:T(8,128)S(1)} async-done(((f32[64,32,128]{2,1,0:T(8,128)}), f32[64,32,128]{2,1,0:T(8,128)S(1)}, u32[]{:S(2)}, u32[]{:S(2)}) %all-to-all-start.4) | async-done | bytes 1048608 | tf_op jit(solution)/shard_map/all_to_all | solution.py:38
  594.8 1.9 copy.89
  (319 shorter events, 205.0 us)
Async XLA Ops:
  7.2 27.4 %copy-start = (bf16[2048,256]{1,0:T(8,128)(2,1)S(1)}, bf16[2048,256]{1,0:T(8,128)(2,1)}, u32[]{:S(2)}) copy-start(bf16[2048,256]{1,0:T(8,128)(2,1)} %param.21) | copy-start | bytes 3145732
  8.9 23.9 %copy-start.7 = (bf16[128,128]{1,0:T(8,128)(2,1)S(1)}, bf16[128,128]{1,0:T(8,128)(2,1)}, u32[]{:S(2)}) copy-start(bf16[128,128]{1,0:T(8,128)(2,1)} %param.23) | copy-start | bytes 98308
  8.9 23.9 %copy-start.13 = (bf16[128,128]{1,0:T(8,128)(2,1)S(1)}, bf16[128,128]{1,0:T(8,128)(2,1)}, u32[]{:S(2)}) copy-start(bf16[128,128]{1,0:T(8,128)(2,1)} %param.22) | copy-start | bytes 98308
  8.9 24.9 %copy-start.2 = (bf16[32,2048]{1,0:T(8,128)(2,1)S(1)}, bf16[32,2048]{1,0:T(8,128)(2,1)}, u32[]{:S(2)}) copy-start(bf16[32,2048]{1,0:T(8,128)(2,1)} %param.16) | copy-start | bytes 393220
  10.0 24.6 %copy-start.10 = (f32[2048]{0:T(1024)S(1)}, f32[2048]{0:T(1024)}, u32[]{:S(2)}) copy-start(f32[2048]{0:T(1024)} %param.18) | copy-start | bytes 24580
  12.0 22.9 %copy-start.1 = (bf16[2048,256]{1,0:T(8,128)(2,1)S(1)}, bf16[2048,256]{1,0:T(8,128)(2,1)}, u32[]{:S(2)}) copy-start(bf16[2048,256]{1,0:T(8,128)(2,1)} %param.20) | copy-start | bytes 3145732
  13.8 190.4 %all-to-all-start = ((bf16[64,128,128]{2,1,0:T(8,128)(2,1)}), bf16[64,128,128]{2,1,0:T(8,128)(2,1)}, u32[]{:S(2)}, u32[]{:S(2)}) async-start(bf16[64,128,128]{2,1,0:T(8,128)(2,1)} %stack.11), calls=%async_computation | async-start | bytes 4194304 | tf_op jit(solution)/shard_map/all_to_all | solution.py:162
  32.8 165.6 %all-gather.5.cloned.1.call-start = ((), (), s32[]{:S(2)}) async-start(), calls=%async_computation.6 | async-start | bytes 4259840 | tf_op jit(solution)/shard_map/all_gather | solution.py:17
  33.8 365.7 %all-gather.3.cloned.1.call-start = ((), (), s32[]{:S(2)}) async-start(), calls=%async_computation.5 | async-start | bytes 8519680 | tf_op jit(solution)/shard_map/all_gather | solution.py:17
  34.6 13.9 %copy-start.14 = (f32[32]{0:T(128)}, f32[32]{0:T(128)S(1)}, u32[]{:S(2)}) copy-start(f32[32]{0:T(128)S(1)} %fusion.122) | copy-start | bytes 388
  224.8 32.4 %copy-start.12 = (f32[16,512,1]{1,2,0:T(1,128)}, f32[16,512,1]{1,2,0:T(1,128)S(1)}, u32[]{:S(2)}) copy-start(f32[16,512,1]{1,2,0:T(1,128)S(1)} %get-tuple-element.121) | copy-start | bytes 98308
  399.4 5.8 copy-start.4
  399.4 5.8 copy-start.6
  399.4 5.8 copy-start.8
  399.5 5.8 copy-start.17
  405.3 102.7 %copy-start.11 = (f32[2048]{0:T(1024)S(1)}, f32[2048]{0:T(1024)}, u32[]{:S(2)}) copy-start(f32[2048]{0:T(1024)} %param.17) | copy-start | bytes 24580
  488.8 14.6 %all-to-all-start.1 = ((bf16[8,16,2048]{2,1,0:T(8,128)(2,1)}), bf16[8,16,2048]{2,1,0:T(8,128)(2,1)}, u32[]{:S(2)}, u32[]{:S(2)}) async-start(bf16[8,16,2048]{2,1,0:T(8,128)(2,1)} %bitcast.217), calls=%async_computation.1 | async-start | bytes 1048576 | tf_op jit(solution)/shard_map/all_to_all | solution.py:44
  503.4 9.4 %all-to-all-start.3 = ((bf16[8,32,256]{2,1,0:T(8,128)(2,1)}), bf16[8,32,256]{2,1,0:T(8,128)(2,1)S(1)}, u32[]{:S(2)}, u32[]{:S(2)}) async-start(bf16[8,32,256]{2,1,0:T(8,128)(2,1)} %convert_element_type.121), calls=%async_computation.3 | async-start | bytes 262144 | tf_op jit(solution)/shard_map/all_to_all | solution.py:238
  506.8 34.0 %copy-start.3 = (bf16[32,2048]{1,0:T(8,128)(2,1)S(1)}, bf16[32,2048]{1,0:T(8,128)(2,1)}, u32[]{:S(2)}) copy-start(bf16[32,2048]{1,0:T(8,128)(2,1)} %param.16) | copy-start | bytes 393220
  512.8 15.5 %copy-start.9 = (bf16[8,32,256]{2,1,0:T(8,128)(2,1)}, bf16[8,32,256]{2,1,0:T(8,128)(2,1)S(1)}, u32[]{:S(2)}) copy-start(bf16[8,32,256]{2,1,0:T(8,128)(2,1)S(1)} %all-to-all-done.3) | copy-start | bytes 393220
  513.6 27.7 %copy-start.19 = (f32[32]{0:T(128)S(1)}, f32[32]{0:T(128)}, u32[]{:S(2)}) copy-start(f32[32]{0:T(128)} %copy-done.18) | copy-start | bytes 388
  513.6 27.7 %copy-start.15 = (f32[32]{0:T(128)S(1)}, f32[32]{0:T(128)}, u32[]{:S(2)}) copy-start(f32[32]{0:T(128)} %copy-done.14) | copy-start | bytes 388
  513.6 14.6 %all-to-all-start.2 = ((bf16[8,16,2048]{2,1,0:T(8,128)(2,1)}), bf16[8,16,2048]{2,1,0:T(8,128)(2,1)}, u32[]{:S(2)}, u32[]{:S(2)}) async-start(bf16[8,16,2048]{2,1,0:T(8,128)(2,1)} %broadcast_in_dim.22), calls=%async_computation.2 | async-start | bytes 1048576 | tf_op jit(solution)/shard_map/all_to_all | solution.py:56
  528.3 65.9 %all-to-all-start.4 = ((f32[64,32,128]{2,1,0:T(8,128)}), f32[64,32,128]{2,1,0:T(8,128)S(1)}, u32[]{:S(2)}, u32[]{:S(2)}) async-start(f32[64,32,128]{2,1,0:T(8,128)} %fusion.92), calls=%async_computation.4 | async-start | bytes 2097152 | tf_op jit(solution)/shard_map/all_to_all | solution.py:38
  (3 other events, 2.1 us)
Sparse Core Ops, SparseCore 0:
  36.5 161.7 all-gather.4
  201.8 152.1 all-gather.2
